TPU v7x, 32 devices: a whole 2x2x4 slice. The times are simulated.
32 devices in a mesh: kv: 16 (over z, y, x), tp: 2 (over core).
Axes of the slice: x: 2, y: 2, z: 4, core: 2. Of those that a mesh axis runs over, the one named last changes fastest.
Arguments:
- residual_in: bfloat16 [96, 2048], P('kv', 'tp'), may hold values from -36 to 36
- gain_pre: float32 [2048], P('tp'), may hold values from 0.1 to 1.9
- gate_pre: bfloat16 [2048, 5632], P('tp', 'kv'), may hold values from -0.125 to 0.125
- up_pre: bfloat16 [2048, 5632], P('tp', 'kv'), may hold values from -0.125 to 0.125
- down_pre: bfloat16 [5632, 2048], P('kv', 'tp'), may hold values from -0.078125 to 0.078125
- gain_mix: float32 [2048], replicated, may hold values from 0.1 to 1.9
- query_weight: bfloat16 [2048, 2048], P('kv', 'tp'), may hold values from -0.125 to 0.125
- forget_weight: bfloat16 [2048, 2048], P('kv', 'tp'), may hold values from -0.125 to 0.125
- value_weight: bfloat16 [2048, 2048], P('kv', 'tp'), may hold values from -0.125 to 0.125
- outgate_weight: bfloat16 [2048, 2048], P('kv', 'tp'), may hold values from -0.125 to 0.125
- lower_bound: float32 [2048], P('tp'), may hold values from 0.05 to 0.95
- head_gain: float32 [2048], P('tp'), may hold values from 0.1 to 1.9
- out_weight: bfloat16 [2048, 2048], P('tp'), may hold values from -0.125 to 0.125
- gain_post: float32 [2048], P('tp'), may hold values from 0.1 to 1.9
- gate_post: bfloat16 [2048, 5632], P('tp', 'kv'), may hold values from -0.125 to 0.125
- up_post: bfloat16 [2048, 5632], P('tp', 'kv'), may hold values from -0.125 to 0.125
- down_post: bfloat16 [5632, 2048], P('kv', 'tp'), may hold values from -0.078125 to 0.078125
- memory_state: float32 [96, 16, 128, 128], P('kv', 'tp'), may hold values from -4 to 4
Outputs:
- layer_out: bfloat16 [96, 2048], P('kv', 'tp')
- next_state: float32 [96, 16, 128, 128], P('kv', 'tp')
All inputs are finite; a program needn't handle non-finite values.
Results may differ from a plain program's by a relative error of at most 0.014.
Values may be sent and summed in bfloat16 or wider, within the bound.
A program may use at most 64 MiB of HBM per device.

v0:
```python
import jax
import jax.numpy as jnp
from jax import lax
from jax.sharding import PartitionSpec as P

D = 2048
HEAD_DIM = 128
EPSILON = 1e-06


def channel_mixer(row_block, gain_vec, gate_weight, up_weight, down_weight):
    gathered = lax.all_gather(row_block, "kv", axis=0, tiled=True)
    widened = gathered.astype(jnp.float32)
    part_squares = jnp.sum(widened * widened, axis=1)
    scaled = (widened * gain_vec).astype(jnp.bfloat16)
    gate_part = jnp.dot(scaled, gate_weight, preferred_element_type=jnp.float32)
    up_part = jnp.dot(scaled, up_weight, preferred_element_type=jnp.float32)
    gate_share, up_share, square_share = (
        lax.psum_scatter(
            gate_part.astype(jnp.bfloat16), "tp", scatter_dimension=0, tiled=True
        ).astype(jnp.float32),
        lax.psum_scatter(
            up_part.astype(jnp.bfloat16), "tp", scatter_dimension=0, tiled=True
        ).astype(jnp.float32),
        lax.psum_scatter(
            part_squares.astype(jnp.bfloat16), "tp", scatter_dimension=0, tiled=True
        ).astype(jnp.float32),
    )
    share_inverse = lax.rsqrt(square_share / D + EPSILON)[:, None]
    hidden_share = (jax.nn.silu(gate_share * share_inverse) * (up_share * share_inverse)).astype(
        jnp.bfloat16
    )
    hidden = lax.all_gather(hidden_share, "tp", axis=0, tiled=True)
    return lax.psum_scatter(
        jnp.dot(hidden, down_weight, preferred_element_type=jnp.float32),
        "kv",
        scatter_dimension=0,
        tiled=True,
    )


def token_mixer(
    stream_a,
    gain_mix,
    query_weight,
    forget_weight,
    value_weight,
    outgate_weight,
    lower_bound,
    head_gain,
    out_weight,
    memory_state,
):
    full_rows = lax.all_gather(stream_a, "tp", axis=1, tiled=True)
    widened = full_rows.astype(jnp.float32)
    inverse = lax.rsqrt(jnp.mean(widened * widened, axis=1, keepdims=True) + EPSILON)
    scaled = (widened * gain_mix).astype(jnp.bfloat16)
    weights = (query_weight, forget_weight, value_weight, outgate_weight)
    blocks = lax.all_to_all(scaled, "kv", split_axis=1, concat_axis=0, tiled=True)
    joined = jnp.concatenate(weights, axis=1)
    projected = lax.psum_scatter(
        jnp.dot(blocks, joined, preferred_element_type=jnp.float32),
        "kv",
        scatter_dimension=0,
        tiled=True,
    )
    projected = projected * inverse
    seq_rows = scaled.shape[0]
    local_heads = query_weight.shape[1] // HEAD_DIM
    reshaped = projected.reshape(seq_rows, 4, local_heads, HEAD_DIM)
    query_pre = reshaped[:, 0]
    forget_pre = reshaped[:, 1]
    value_pre = reshaped[:, 2]
    outgate_pre = reshaped[:, 3]
    floor_rate = lower_bound.reshape(local_heads, HEAD_DIM)
    log_keep = jnp.logaddexp(
        jnp.log(floor_rate), jnp.log1p(-floor_rate) + jax.nn.log_sigmoid(forget_pre)
    )
    inject = (1.0 - floor_rate) * jax.nn.sigmoid(-forget_pre)
    next_state = (
        jnp.exp(log_keep)[..., None] * memory_state + inject[..., None] * value_pre[:, :, None, :]
    )
    readout = jnp.einsum(
        "bhk,bhkv->bhv", jax.nn.silu(query_pre), next_state, precision=lax.Precision.HIGHEST
    )
    normed = (
        readout
        * lax.rsqrt(jnp.mean(readout * readout, axis=2, keepdims=True) + EPSILON)
        * head_gain.reshape(local_heads, HEAD_DIM)
    )
    mixed_heads = (
        (normed * jax.nn.silu(outgate_pre))
        .reshape(seq_rows, local_heads * HEAD_DIM)
        .astype(jnp.bfloat16)
    )
    partial_out = jnp.dot(mixed_heads, out_weight, preferred_element_type=jnp.float32)
    mixed = lax.psum_scatter(
        partial_out.astype(jnp.bfloat16), "tp", scatter_dimension=1, tiled=True
    ).astype(jnp.float32)
    return (mixed, next_state)


def shards(
    residual_in,
    gain_pre,
    gate_pre,
    up_pre,
    down_pre,
    gain_mix,
    query_weight,
    forget_weight,
    value_weight,
    outgate_weight,
    lower_bound,
    head_gain,
    out_weight,
    gain_post,
    gate_post,
    up_post,
    down_post,
    memory_state,
):
    branch_a = channel_mixer(residual_in, gain_pre, gate_pre, up_pre, down_pre)
    stream_a = (residual_in.astype(jnp.float32) + 0.5 * branch_a).astype(jnp.bfloat16)
    mixed, next_state = token_mixer(
        stream_a,
        gain_mix,
        query_weight,
        forget_weight,
        value_weight,
        outgate_weight,
        lower_bound,
        head_gain,
        out_weight,
        memory_state,
    )
    stream_b = (stream_a.astype(jnp.float32) + mixed).astype(jnp.bfloat16)
    branch_b = channel_mixer(stream_b, gain_post, gate_post, up_post, down_post)
    layer_out = (stream_b.astype(jnp.float32) + 0.5 * branch_b).astype(jnp.bfloat16)
    return (layer_out, next_state)


def solution(mesh):
    in_specs = (
        P("kv", "tp"),
        P("tp"),
        P("tp", "kv"),
        P("tp", "kv"),
        P("kv", "tp"),
        P(),
        P("kv", "tp"),
        P("kv", "tp"),
        P("kv", "tp"),
        P("kv", "tp"),
        P("tp"),
        P("tp"),
        P("tp", None),
        P("tp"),
        P("tp", "kv"),
        P("tp", "kv"),
        P("kv", "tp"),
        P("kv", "tp", None, None),
    )
    out_specs = (P("kv", "tp"), P("kv", "tp", None, None))
    return jax.shard_map(shards, mesh=mesh, in_specs=in_specs, out_specs=out_specs, check_vma=False)
```

profile of v0, /device:TPU:18, one launch (start us, length us, event | category | flops | bytes accessed | tf_op | source)
XLA Modules:
  0.0 353.3 jit_solution(17581845288127005112)
XLA Ops:
  7.3 30.5 %all-gather = bf16[16,6,1024]{2,1,0:T(8,128)(2,1)S(1)} all-gather(bf16[1,6,1024]{2,1,0:T(8,128)(2,1)} %bitcast.90), channel_id=1, replica_groups=mesh['kv'=16,'tp'=2] {'kv'}, dimensions={0}, use_global_device_ids=true | all-gather | bytes 208896 | tf_op jit(solution)/shard_map/all_gather | solution.py:12
  37.8 0.1 reshape.102
  37.9 2.2 convolution_convert_fusion.4
  40.1 0.0 reduce-scatter.14.cloned.1.call-start
  40.2 2.1 convolution_convert_fusion.3
  42.3 0.1 multiply_reduce_fusion.1
  42.4 0.6 dynamic-slice
  43.7 2.5 all-reduce
  46.1 0.1 fusion.33
  46.2 9.6 %reduce-scatter.12.cloned.1.call-done = bf16[48,352]{1,0:T(8,128)(2,1)} async-done(((bf16[96,352]{1,0:T(8,128)(2,1)}), bf16[48,352]{1,0:T(8,128)(2,1)}) %reduce-scatter.12.cloned.1.call-update) | async-done | bytes 33808 | tf_op jit(solution)/shard_map/reduce_scatter | solution.py:19
  55.8 11.4 %reduce-scatter.14.cloned.1.call-done = bf16[48,352]{1,0:T(8,128)(2,1)} async-done(((bf16[96,352]{1,0:T(8,128)(2,1)}), bf16[48,352]{1,0:T(8,128)(2,1)}) %reduce-scatter.14.cloned.1.call-update) | async-done | bytes 33808 | tf_op jit(solution)/shard_map/reduce_scatter | solution.py:22
  67.3 0.9 multiply_convert_fusion.3
  68.2 1.9 all_gather.16
  70.1 0.3 fusion.36
  70.3 35.6 %fusion = f32[8,1024]{1,0:T(8,128)S(1)} fusion(f32[96,1024]{1,0:T(8,128)S(1)} %fusion.36), kind=kCustom, calls=%all-reduce-scatter | all-reduce-scatter fusion | flops 131073 | bytes 426496
  105.9 6.0 %collective-permute-start.2 = (f32[8,1024]{1,0:T(8,128)S(1)}, f32[8,1024]{1,0:T(8,128)S(1)}, u32[]{:S(2)}, u32[]{:S(2)}) collective-permute-start(f32[8,1024]{1,0:T(8,128)S(1)} %fusion), channel_id=1, source_target_pairs={{0,6},{2,8},{4,10},{6,12},{8,14},{10,16},{12,18},{14,20},{16,22},{... | collective-permute-start | bytes 98312
  111.9 4.4 %collective-permute-start.1 = (f32[8,1024]{1,0:T(8,128)S(1)}, f32[8,1024]{1,0:T(8,128)S(1)}, u32[]{:S(2)}, u32[]{:S(2)}) collective-permute-start(f32[8,1024]{1,0:T(8,128)S(1)} %fusion), channel_id=1, source_target_pairs={{0,4},{2,6},{4,8},{6,10},{8,12},{10,14},{12,16},{14,18},{16,20},{1... | collective-permute-start | bytes 98312
  116.3 4.9 %collective-permute-start = (f32[8,1024]{1,0:T(8,128)S(1)}, f32[8,1024]{1,0:T(8,128)S(1)}, u32[]{:S(2)}, u32[]{:S(2)}) collective-permute-start(f32[8,1024]{1,0:T(8,128)S(1)} %fusion), channel_id=1, source_target_pairs={{0,2},{2,4},{4,6},{6,8},{8,10},{10,12},{12,14},{14,16},{16,18},{18... | collective-permute-start | bytes 98312
  121.2 1.9 collective-permute-start.3
  123.1 0.6 dynamic-slice.12
  124.4 2.6 collective-permute-done.3
  127.0 0.4 concatenate.4
  127.5 1.8 all_gather.17
  129.3 0.7 fusion.13
  130.1 5.1 %all-to-all-start = ((bf16[6,16,128]{2,0,1:T(8,128)(2,1)}), bf16[6,16,128]{2,0,1:T(8,128)(2,1)S(1)}, u32[]{:S(2)}, u32[]{:S(2)}) async-start(bf16[6,16,128]{2,0,1:T(8,128)(2,1)} %get-tuple-element.6), calls=%async_computation.2 | async-start | bytes 65536 | tf_op jit(solution)/shard_map/all_to_all | solution.py:59
  135.3 4.3 %all-to-all-done = bf16[6,16,128]{2,0,1:T(8,128)(2,1)S(1)} async-done(((bf16[6,16,128]{2,0,1:T(8,128)(2,1)}), bf16[6,16,128]{2,0,1:T(8,128)(2,1)S(1)}, u32[]{:S(2)}, u32[]{:S(2)}) %all-to-all-start) | async-done | bytes 24608 | tf_op jit(solution)/shard_map/all_to_all | solution.py:59
  139.6 0.4 fusion.3
  139.9 52.3 %fusion.1 = f32[8,4096]{1,0:T(8,128)S(1)} fusion(f32[96,4096]{1,0:T(8,128)S(1)} %fusion.3), kind=kCustom, calls=%all-reduce-scatter.1 | all-reduce-scatter fusion | flops 524289 | bytes 1704448
  192.3 3.3 collective-permute-start.6
  195.5 3.0 collective-permute-start.5
  198.5 3.5 collective-permute-start.4
  202.0 1.9 collective-permute-start.7
  204.0 4.9 %collective-permute-done.7 = f32[6,4096]{1,0:T(8,128)S(1)} collective-permute-done((f32[6,4096]{1,0:T(8,128)S(1)}, f32[6,4096]{1,0:T(8,128)S(1)}, u32[]{:S(2)}, u32[]{:S(2)}) %collective-permute-start.7) | collective-permute-done | bytes 98336
  208.9 0.8 concatenate.5
  209.7 0.1 fusion.11
  209.8 0.1 select_exponential_fusion
  209.9 4.0 %multiply_add_fusion = f32[6,8,128,128]{3,2,1,0:T(8,128)S(1)} fusion(f32[6,8,128,128]{3,2,1,0:T(8,128)} %param.35, f32[6,8,128]{2,1,0:T(8,128)S(1)} %slice_bitcast_fusion.1, f32[6,8,128]{2,1,0:T(8,128)S(1)} %get-tuple-element.3, f32[6,8,128]{2,1,0:T(8,128)S(1)} %get-tuple-element.2), kind=kLoop, calls=%fused_computation | loop fusion | flops 2359296 | bytes 6365184 | tf_op jit(solution)/shard_map/add | solution.py:81
  213.9 1.6 copy-done.1
  215.6 2.8 fusion.37
  218.3 0.1 multiply_reduce_fusion.2
  218.4 0.1 fusion.27
  218.5 1.3 convolution_convert_fusion
  219.9 7.1 %reduce-scatter.16.cloned.1.call-done = bf16[6,1024]{1,0:T(8,128)(2,1)} async-done(((bf16[6,2048]{1,0:T(8,128)(2,1)}), bf16[6,1024]{1,0:T(8,128)(2,1)}) %reduce-scatter.16.cloned.1.call-update) | async-done | bytes 12304 | tf_op jit(solution)/shard_map/reduce_scatter | solution.py:97
  226.9 0.7 fusion.28
  227.7 30.4 %all-gather.1 = bf16[16,6,1024]{2,1,0:T(8,128)(2,1)S(1)} all-gather(bf16[1,6,1024]{2,1,0:T(8,128)(2,1)S(1)} %fusion.28), channel_id=1, replica_groups=mesh['kv'=16,'tp'=2] {'kv'}, dimensions={0}, use_global_device_ids=true | all-gather | bytes 208896 | tf_op jit(solution)/shard_map/all_gather | solution.py:12
  258.1 0.1 reshape.103
  258.1 1.7 convolution_convert_fusion.2
  259.9 1.7 convolution_convert_fusion.1
  261.6 0.1 multiply_reduce_fusion
  261.7 2.5 all-reduce.3
  264.2 0.1 fusion.34
  264.3 11.0 %reduce-scatter.18.cloned.1.call-done = bf16[48,352]{1,0:T(8,128)(2,1)} async-done(((bf16[96,352]{1,0:T(8,128)(2,1)}), bf16[48,352]{1,0:T(8,128)(2,1)}) %reduce-scatter.18.cloned.1.call-update) | async-done | bytes 33808 | tf_op jit(solution)/shard_map/reduce_scatter | solution.py:19
  275.3 10.7 %reduce-scatter.20.cloned.1.call-done = bf16[48,352]{1,0:T(8,128)(2,1)} async-done(((bf16[96,352]{1,0:T(8,128)(2,1)}), bf16[48,352]{1,0:T(8,128)(2,1)}) %reduce-scatter.20.cloned.1.call-update) | async-done | bytes 33808 | tf_op jit(solution)/shard_map/reduce_scatter | solution.py:22
  286.0 0.9 multiply_convert_fusion.2
  286.9 1.9 all_gather.19
  288.8 0.3 fusion.38
  289.1 35.5 %fusion.2 = f32[8,1024]{1,0:T(8,128)S(1)} fusion(f32[96,1024]{1,0:T(8,128)S(1)} %fusion.38), kind=kCustom, calls=%all-reduce-scatter.2 | all-reduce-scatter fusion | flops 131073 | bytes 426496
  324.6 6.1 %collective-permute-start.10 = (f32[8,1024]{1,0:T(8,128)S(1)}, f32[8,1024]{1,0:T(8,128)S(1)}, u32[]{:S(2)}, u32[]{:S(2)}) collective-permute-start(f32[8,1024]{1,0:T(8,128)S(1)} %fusion.2), channel_id=1, source_target_pairs={{0,6},{2,8},{4,10},{6,12},{8,14},{10,16},{12,18},{14,20},{16,22},{... | collective-permute-start | bytes 98312
  330.6 4.4 %collective-permute-start.9 = (f32[8,1024]{1,0:T(8,128)S(1)}, f32[8,1024]{1,0:T(8,128)S(1)}, u32[]{:S(2)}, u32[]{:S(2)}) collective-permute-start(f32[8,1024]{1,0:T(8,128)S(1)} %fusion.2), channel_id=1, source_target_pairs={{0,4},{2,6},{4,8},{6,10},{8,12},{10,14},{12,16},{14,18},{16,20},{1... | collective-permute-start | bytes 98312
  335.0 4.9 %collective-permute-start.8 = (f32[8,1024]{1,0:T(8,128)S(1)}, f32[8,1024]{1,0:T(8,128)S(1)}, u32[]{:S(2)}, u32[]{:S(2)}) collective-permute-start(f32[8,1024]{1,0:T(8,128)S(1)} %fusion.2), channel_id=1, source_target_pairs={{0,2},{2,4},{4,6},{6,8},{8,10},{10,12},{12,14},{14,16},{16,18},{18... | collective-permute-start | bytes 98312
  339.9 1.9 collective-permute-start.11
  341.8 3.9 %collective-permute-done.11 = f32[6,1024]{1,0:T(8,128)S(1)} collective-permute-done((f32[6,1024]{1,0:T(8,128)S(1)}, f32[6,1024]{1,0:T(8,128)S(1)}, u32[]{:S(2)}, u32[]{:S(2)}) %collective-permute-start.11) | collective-permute-done | bytes 24608
  345.7 0.4 concatenate.6
  346.2 0.6 fusion.16
  (61 shorter events, 0.5 us)
Async XLA Ops:
  7.2 62.9 %copy-start = (bf16[352,1024]{1,0:T(8,128)(2,1)S(1)}, bf16[352,1024]{1,0:T(8,128)(2,1)}, u32[]{:S(2)}) copy-start(bf16[352,1024]{1,0:T(8,128)(2,1)} %param.22) | copy-start | bytes 2162692
  7.2 35.2 %copy-start.16 = (u32[32]{0:T(128)S(1)}, u32[32]{0:T(128)}, u32[]{:S(2)}) copy-start(u32[32]{0:T(128)} %constant.33) | copy-start | bytes 388
  7.2 115.9 %copy-start.11 = (u32[32]{0:T(128)S(1)}, u32[32]{0:T(128)}, u32[]{:S(2)}) copy-start(u32[32]{0:T(128)} %constant.37) | copy-start | bytes 388
  7.2 120.3 %copy-start.6 = (bf16[6,1024]{1,0:T(8,128)(2,1)S(1)}, bf16[6,1024]{1,0:T(8,128)(2,1)}, u32[]{:S(2)}) copy-start(bf16[6,1024]{1,0:T(8,128)(2,1)} %param.18) | copy-start | bytes 36868
  7.2 122.1 %copy-start.8 = (f32[2048]{0:T(1024)S(1)}, f32[2048]{0:T(1024)}, u32[]{:S(2)}) copy-start(f32[2048]{0:T(1024)} %param.23) | copy-start | bytes 24580
  7.2 48.6 %reduce-scatter.12.cloned.1.call-start = ((), (), s32[]{:S(2)}) async-start(), calls=%async_computation.6 | async-start | bytes 110592 | tf_op jit(solution)/shard_map/reduce_scatter | solution.py:19
  7.3 128.0 %copy-start.10 = (f32[1024]{0:T(1024)S(1)}, f32[1024]{0:T(1024)}, u32[]{:S(2)}) copy-start(f32[1024]{0:T(1024)} %param.28) | copy-start | bytes 12292
  37.8 101.7 %copy-start.12 = (bf16[128,1024]{1,0:T(8,128)(2,1)S(1)}, bf16[128,1024]{1,0:T(8,128)(2,1)}, u32[]{:S(2)}) copy-start(bf16[128,1024]{1,0:T(8,128)(2,1)} %param.27) | copy-start | bytes 786436
  37.8 101.7 %copy-start.13 = (bf16[128,1024]{1,0:T(8,128)(2,1)S(1)}, bf16[128,1024]{1,0:T(8,128)(2,1)}, u32[]{:S(2)}) copy-start(bf16[128,1024]{1,0:T(8,128)(2,1)} %param.26) | copy-start | bytes 786436
  37.8 101.7 %copy-start.14 = (bf16[128,1024]{1,0:T(8,128)(2,1)S(1)}, bf16[128,1024]{1,0:T(8,128)(2,1)}, u32[]{:S(2)}) copy-start(bf16[128,1024]{1,0:T(8,128)(2,1)} %param.25) | copy-start | bytes 786436
  37.8 101.7 %copy-start.15 = (bf16[128,1024]{1,0:T(8,128)(2,1)S(1)}, bf16[128,1024]{1,0:T(8,128)(2,1)}, u32[]{:S(2)}) copy-start(bf16[128,1024]{1,0:T(8,128)(2,1)} %param.24) | copy-start | bytes 786436
  40.1 27.2 %reduce-scatter.14.cloned.1.call-start = ((), (), s32[]{:S(2)}) async-start(), calls=%async_computation.7 | async-start | bytes 110592 | tf_op jit(solution)/shard_map/reduce_scatter | solution.py:22
  105.9 21.1 %collective-permute-start.2 = (f32[8,1024]{1,0:T(8,128)S(1)}, f32[8,1024]{1,0:T(8,128)S(1)}, u32[]{:S(2)}, u32[]{:S(2)}) collective-permute-start(f32[8,1024]{1,0:T(8,128)S(1)} %fusion), channel_id=1, source_target_pairs={{0,6},{2,8},{4,10},{6,12},{8,14},{10,16},{12,18},{14,20},{16,22},{... | collective-permute-start | bytes 98312
  111.9 15.1 %collective-permute-start.1 = (f32[8,1024]{1,0:T(8,128)S(1)}, f32[8,1024]{1,0:T(8,128)S(1)}, u32[]{:S(2)}, u32[]{:S(2)}) collective-permute-start(f32[8,1024]{1,0:T(8,128)S(1)} %fusion), channel_id=1, source_target_pairs={{0,4},{2,6},{4,8},{6,10},{8,12},{10,14},{12,16},{14,18},{16,20},{1... | collective-permute-start | bytes 98312
  116.3 10.7 %collective-permute-start = (f32[8,1024]{1,0:T(8,128)S(1)}, f32[8,1024]{1,0:T(8,128)S(1)}, u32[]{:S(2)}, u32[]{:S(2)}) collective-permute-start(f32[8,1024]{1,0:T(8,128)S(1)} %fusion), channel_id=1, source_target_pairs={{0,2},{2,4},{4,6},{6,8},{8,10},{10,12},{12,14},{14,16},{16,18},{18... | collective-permute-start | bytes 98312
  121.2 5.8 %collective-permute-start.3 = (f32[6,1024]{1,0:T(8,128)S(1)}, f32[6,1024]{1,0:T(8,128)S(1)}, u32[]{:S(2)}, u32[]{:S(2)}) collective-permute-start(f32[6,1024]{1,0:T(8,128)S(1)} %slice.20), channel_id=1, source_target_pairs={{0,8},{2,10},{4,12},{6,14},{8,16},{10,18},{12,20},{14,22},{16,24},... | collective-permute-start | bytes 73736
  130.1 9.4 %all-to-all-start = ((bf16[6,16,128]{2,0,1:T(8,128)(2,1)}), bf16[6,16,128]{2,0,1:T(8,128)(2,1)S(1)}, u32[]{:S(2)}, u32[]{:S(2)}) async-start(bf16[6,16,128]{2,0,1:T(8,128)(2,1)} %get-tuple-element.6), calls=%async_computation.2 | async-start | bytes 65536 | tf_op jit(solution)/shard_map/all_to_all | solution.py:59
  135.2 91.8 %reduce-scatter.16.cloned.1.call-start = ((), (), s32[]{:S(2)}) async-start(), calls=%async_computation.8 | async-start | bytes 49152 | tf_op jit(solution)/shard_map/reduce_scatter | solution.py:97
  192.3 16.6 %collective-permute-start.6 = (f32[8,4096]{1,0:T(8,128)S(1)}, f32[8,4096]{1,0:T(8,128)S(1)}, u32[]{:S(2)}, u32[]{:S(2)}) collective-permute-start(f32[8,4096]{1,0:T(8,128)S(1)} %fusion.1), channel_id=1, source_target_pairs={{0,6},{2,8},{4,10},{6,12},{8,14},{10,16},{12,18},{14,20},{16,22},{... | collective-permute-start | bytes 393224
  195.5 13.4 %collective-permute-start.5 = (f32[8,4096]{1,0:T(8,128)S(1)}, f32[8,4096]{1,0:T(8,128)S(1)}, u32[]{:S(2)}, u32[]{:S(2)}) collective-permute-start(f32[8,4096]{1,0:T(8,128)S(1)} %fusion.1), channel_id=1, source_target_pairs={{0,4},{2,6},{4,8},{6,10},{8,12},{10,14},{12,16},{14,18},{16,20},{1... | collective-permute-start | bytes 393224
  198.5 10.4 %collective-permute-start.4 = (f32[8,4096]{1,0:T(8,128)S(1)}, f32[8,4096]{1,0:T(8,128)S(1)}, u32[]{:S(2)}, u32[]{:S(2)}) collective-permute-start(f32[8,4096]{1,0:T(8,128)S(1)} %fusion.1), channel_id=1, source_target_pairs={{0,2},{2,4},{4,6},{6,8},{8,10},{10,12},{12,14},{14,16},{16,18},{18... | collective-permute-start | bytes 393224
  202.0 6.9 %collective-permute-start.7 = (f32[6,4096]{1,0:T(8,128)S(1)}, f32[6,4096]{1,0:T(8,128)S(1)}, u32[]{:S(2)}, u32[]{:S(2)}) collective-permute-start(f32[6,4096]{1,0:T(8,128)S(1)} %slice.21), channel_id=1, source_target_pairs={{0,8},{2,10},{4,12},{6,14},{8,16},{10,18},{12,20},{14,22},{16,24},... | collective-permute-start | bytes 294920
  209.9 8.6 %copy-start.2 = (bf16[1024,2048]{1,0:T(8,128)(2,1)S(1)}, bf16[1024,2048]{1,0:T(8,128)(2,1)}, u32[]{:S(2)}) copy-start(bf16[1024,2048]{1,0:T(8,128)(2,1)} %param.30) | copy-start | bytes 12582916
  213.9 1.7 copy-start.1
  213.9 4.5 %copy-start.9 = (f32[1024]{0:T(1024)S(1)}, f32[1024]{0:T(1024)}, u32[]{:S(2)}) copy-start(f32[1024]{0:T(1024)} %param.29) | copy-start | bytes 12292
  218.3 39.8 %copy-start.3 = (bf16[1024,352]{0,1:T(8,128)(2,1)S(1)}, bf16[1024,352]{0,1:T(8,128)(2,1)}, u32[]{:S(2)}) copy-start(bf16[1024,352]{0,1:T(8,128)(2,1)} %param.32) | copy-start | bytes 2162692
  218.5 41.4 %copy-start.4 = (bf16[1024,352]{0,1:T(8,128)(2,1)S(1)}, bf16[1024,352]{0,1:T(8,128)(2,1)}, u32[]{:S(2)}) copy-start(bf16[1024,352]{0,1:T(8,128)(2,1)} %param.33) | copy-start | bytes 2162692
  219.8 69.0 %copy-start.5 = (bf16[352,1024]{1,0:T(8,128)(2,1)S(1)}, bf16[352,1024]{1,0:T(8,128)(2,1)}, u32[]{:S(2)}) copy-start(bf16[352,1024]{1,0:T(8,128)(2,1)} %param.34) | copy-start | bytes 2162692
  219.8 55.5 %reduce-scatter.18.cloned.1.call-start = ((), (), s32[]{:S(2)}) async-start(), calls=%async_computation.9 | async-start | bytes 110592 | tf_op jit(solution)/shard_map/reduce_scatter | solution.py:19
  258.1 88.0 %copy-start.7 = (bf16[6,1024]{1,0:T(8,128)(2,1)S(1)}, bf16[6,1024]{1,0:T(8,128)(2,1)}, u32[]{:S(2)}) copy-start(bf16[6,1024]{1,0:T(8,128)(2,1)} %reduce-scatter.16.cloned.1.call-done) | copy-start | bytes 36868
  259.8 26.2 %reduce-scatter.20.cloned.1.call-start = ((), (), s32[]{:S(2)}) async-start(), calls=%async_computation.10 | async-start | bytes 110592 | tf_op jit(solution)/shard_map/reduce_scatter | solution.py:22
  324.6 21.1 %collective-permute-start.10 = (f32[8,1024]{1,0:T(8,128)S(1)}, f32[8,1024]{1,0:T(8,128)S(1)}, u32[]{:S(2)}, u32[]{:S(2)}) collective-permute-start(f32[8,1024]{1,0:T(8,128)S(1)} %fusion.2), channel_id=1, source_target_pairs={{0,6},{2,8},{4,10},{6,12},{8,14},{10,16},{12,18},{14,20},{16,22},{... | collective-permute-start | bytes 98312
  330.6 15.1 %collective-permute-start.9 = (f32[8,1024]{1,0:T(8,128)S(1)}, f32[8,1024]{1,0:T(8,128)S(1)}, u32[]{:S(2)}, u32[]{:S(2)}) collective-permute-start(f32[8,1024]{1,0:T(8,128)S(1)} %fusion.2), channel_id=1, source_target_pairs={{0,4},{2,6},{4,8},{6,10},{8,12},{10,14},{12,16},{14,18},{16,20},{1... | collective-permute-start | bytes 98312
  335.0 10.7 %collective-permute-start.8 = (f32[8,1024]{1,0:T(8,128)S(1)}, f32[8,1024]{1,0:T(8,128)S(1)}, u32[]{:S(2)}, u32[]{:S(2)}) collective-permute-start(f32[8,1024]{1,0:T(8,128)S(1)} %fusion.2), channel_id=1, source_target_pairs={{0,2},{2,4},{4,6},{6,8},{8,10},{10,12},{12,14},{14,16},{16,18},{18... | collective-permute-start | bytes 98312
  339.9 5.8 %collective-permute-start.11 = (f32[6,1024]{1,0:T(8,128)S(1)}, f32[6,1024]{1,0:T(8,128)S(1)}, u32[]{:S(2)}, u32[]{:S(2)}) collective-permute-start(f32[6,1024]{1,0:T(8,128)S(1)} %slice.22), channel_id=1, source_target_pairs={{0,8},{2,10},{4,12},{6,14},{8,16},{10,18},{12,20},{14,22},{16,24},... | collective-permute-start | bytes 73736
Sparse Core Ops, SparseCore 0:
  40.2 15.5 reduce-scatter.11
  58.6 8.6 reduce-scatter.13
  219.9 6.9 reduce-scatter.15
  260.0 15.2 reduce-scatter.17
  277.3 8.6 reduce-scatter.19
where the time goes:
time: 354 us; the launch traced here: 353 us
  blocking collectives  195 us (55%)
  waiting for transfers between devices  65.7 us (19%)
  starting transfers between devices  51.3 us (14%)
  between operations  15.6 us (4%)
  matrix products  12.6 us (4%)
  other arithmetic  8.58 us (2%)
  local copies, waits for them, and re-layouts  4.76 us (1%)
    unnamed x5, blocking collectives  128 us
    all_gather x2, blocking collectives, channel_mixer(): gathered = lax.all_gather(row_block, 'kv', axis=0, tiled=True)  60.9 us
    unnamed x12, starting transfers between devices  46 us
    reduce_scatter x2, waiting for transfers between devices, channel_mixer(): lax.psum_scatter(up_part.astype(jnp.bfloat16), 'tp', scatter_dimension=0,...  22.2 us
    reduce_scatter x2, waiting for transfers between devices, channel_mixer(): lax.psum_scatter(gate_part.astype(jnp.bfloat16), 'tp', scatter_dimension=...  20.7 us
    unnamed x17, waiting for transfers between devices  11.5 us
  transfers between devices with their start and end apart: 18, of which 9 were waited for; matrix products, arithmetic and copies ran while one was open for 2% of the time, Pallas kernels for 0%

commit v1 on v0

--- a/solution.py
+++ b/solution.py
@@ -9,7 +9,12 @@
 
 
 def channel_mixer(row_block, gain_vec, gate_weight, up_weight, down_weight):
-    gathered = lax.all_gather(row_block, "kv", axis=0, tiled=True)
+    ring = [row_block]
+    for hop in range(15):
+        ring.append(lax.ppermute(ring[-1], "kv", [(dev, (dev + 1) % 16) for dev in range(16)]))
+    gathered = jnp.roll(
+        jnp.concatenate(ring[::-1], axis=0), (lax.axis_index("kv") + 1) * ring[0].shape[0], axis=0
+    )
     widened = gathered.astype(jnp.float32)
     part_squares = jnp.sum(widened * widened, axis=1)
     scaled = (widened * gain_vec).astype(jnp.bfloat16)

time: 354 us -> 493 us (1.39)
  waiting for transfers between devices: 65.7 us -> 237 us
  blocking collectives: 195 us -> 134 us
  starting transfers between devices: 51.3 us -> 76.9 us
    ppermute x0 -> x30, waiting for transfers between devices: none -> 134 us  [channel_mixer(): lax.ppermute(ring[-1], 'kv', [(dev, (dev + 1) % 16) for dev in range(16)])]
    all_gather x2 -> x0, blocking collectives: 60.9 us -> none  [channel_mixer(): gathered = lax.all_gather(row_block, 'kv', axis=0, tiled=True)]
    reduce_scatter x2, waiting for transfers between devices: 20.7 us -> 57.3 us  [channel_mixer(): lax.psum_scatter(gate_part.astype(jnp.bfloat16), 'tp', scatter_dimension=...]
    ppermute x0 -> x30, starting transfers between devices: none -> 25.6 us  [channel_mixer(): lax.ppermute(ring[-1], 'kv', [(dev, (dev + 1) % 16) for dev in range(16)])]
  transfers between devices with their start and end apart: 18 -> 48, of which waited for: 9 -> 39; matrix products, arithmetic and copies ran while one was open for 2% -> 1% of each run, Pallas kernels for 0% -> 0%
where the time goes in v1:
time: 493 us; the launch traced here: 492 us
  waiting for transfers between devices  237 us (48%)
  blocking collectives  134 us (27%)
  starting transfers between devices  76.9 us (16%)
  between operations  15.6 us (3%)
  matrix products  12.2 us (2%)
  other arithmetic  8.88 us (2%)
  local copies, waits for them, and re-layouts  7.96 us (2%)
    ppermute x30, waiting for transfers between devices, channel_mixer(): lax.ppermute(ring[-1], 'kv', [(dev, (dev + 1) % 16) for dev in range(16)])  134 us
    unnamed x5, blocking collectives  128 us
    reduce_scatter x2, waiting for transfers between devices, channel_mixer(): lax.psum_scatter(gate_part.astype(jnp.bfloat16), 'tp', scatter_dimension=...  57.3 us
    unnamed x12, starting transfers between devices  45.9 us
    ppermute x30, starting transfers between devices, channel_mixer(): lax.ppermute(ring[-1], 'kv', [(dev, (dev + 1) % 16) for dev in range(16)])  25.6 us
    reduce_scatter x2, waiting for transfers between devices, channel_mixer(): lax.psum_scatter(up_part.astype(jnp.bfloat16), 'tp', scatter_dimension=0,...  22.2 us
    unnamed x17, waiting for transfers between devices  11.5 us
  transfers between devices with their start and end apart: 48, of which 39 were waited for; matrix products, arithmetic and copies ran while one was open for 1% of the time, Pallas kernels for 0%

profile of v1, /device:TPU:18, one launch (start us, length us, event | category | flops | bytes accessed | tf_op | source)
XLA Modules:
  0.0 492.1 jit_solution(15458967305459657561)
XLA Ops:
  8.8 2.5 collective-permute-done
  11.3 2.4 collective-permute-start.1
  15.3 3.0 collective-permute-start.2
  18.3 2.6 collective-permute-done.2
  20.9 2.2 collective-permute-start.3
  23.1 3.4 collective-permute-done.3
  27.7 4.2 collective-permute-done.4
  32.4 5.1 %collective-permute-done.5 = bf16[6,1024]{1,0:T(8,128)(2,1)S(1)} collective-permute-done((bf16[6,1024]{1,0:T(8,128)(2,1)S(1)}, bf16[6,1024]{1,0:T(8,128)(2,1)S(1)}, u32[]{:S(2)}, u32[]{:S(2)}) %collective-permute-start.5) | collective-permute-done | bytes 12320 | tf_op jit(solution)/shard_map/ppermute | solution.py:14
  37.5 5.5 %collective-permute-done.6 = bf16[6,1024]{1,0:T(8,128)(2,1)S(1)} collective-permute-done((bf16[6,1024]{1,0:T(8,128)(2,1)S(1)}, bf16[6,1024]{1,0:T(8,128)(2,1)S(1)}, u32[]{:S(2)}, u32[]{:S(2)}) %collective-permute-start.6) | collective-permute-done | bytes 12320 | tf_op jit(solution)/shard_map/ppermute | solution.py:14
  43.0 5.6 %collective-permute-done.7 = bf16[6,1024]{1,0:T(8,128)(2,1)S(1)} collective-permute-done((bf16[6,1024]{1,0:T(8,128)(2,1)S(1)}, bf16[6,1024]{1,0:T(8,128)(2,1)S(1)}, u32[]{:S(2)}, u32[]{:S(2)}) %collective-permute-start.7) | collective-permute-done | bytes 12320 | tf_op jit(solution)/shard_map/ppermute | solution.py:14
  48.6 5.5 %collective-permute-done.8 = bf16[6,1024]{1,0:T(8,128)(2,1)S(1)} collective-permute-done((bf16[6,1024]{1,0:T(8,128)(2,1)S(1)}, bf16[6,1024]{1,0:T(8,128)(2,1)S(1)}, u32[]{:S(2)}, u32[]{:S(2)}) %collective-permute-start.8) | collective-permute-done | bytes 12320 | tf_op jit(solution)/shard_map/ppermute | solution.py:14
  54.1 5.5 %collective-permute-done.9 = bf16[6,1024]{1,0:T(8,128)(2,1)S(1)} collective-permute-done((bf16[6,1024]{1,0:T(8,128)(2,1)S(1)}, bf16[6,1024]{1,0:T(8,128)(2,1)S(1)}, u32[]{:S(2)}, u32[]{:S(2)}) %collective-permute-start.9) | collective-permute-done | bytes 12320 | tf_op jit(solution)/shard_map/ppermute | solution.py:14
  59.6 5.5 %collective-permute-done.10 = bf16[6,1024]{1,0:T(8,128)(2,1)S(1)} collective-permute-done((bf16[6,1024]{1,0:T(8,128)(2,1)S(1)}, bf16[6,1024]{1,0:T(8,128)(2,1)S(1)}, u32[]{:S(2)}, u32[]{:S(2)}) %collective-permute-start.10) | collective-permute-done | bytes 12320 | tf_op jit(solution)/shard_map/ppermute | solution.py:14
  65.2 5.5 %collective-permute-done.11 = bf16[6,1024]{1,0:T(8,128)(2,1)S(1)} collective-permute-done((bf16[6,1024]{1,0:T(8,128)(2,1)S(1)}, bf16[6,1024]{1,0:T(8,128)(2,1)S(1)}, u32[]{:S(2)}, u32[]{:S(2)}) %collective-permute-start.11) | collective-permute-done | bytes 12320 | tf_op jit(solution)/shard_map/ppermute | solution.py:14
  70.7 5.5 %collective-permute-done.12 = bf16[6,1024]{1,0:T(8,128)(2,1)S(1)} collective-permute-done((bf16[6,1024]{1,0:T(8,128)(2,1)S(1)}, bf16[6,1024]{1,0:T(8,128)(2,1)S(1)}, u32[]{:S(2)}, u32[]{:S(2)}) %collective-permute-start.12) | collective-permute-done | bytes 12320 | tf_op jit(solution)/shard_map/ppermute | solution.py:14
  76.5 5.3 %collective-permute-done.13 = bf16[6,1024]{1,0:T(8,128)(2,1)S(1)} collective-permute-done((bf16[6,1024]{1,0:T(8,128)(2,1)S(1)}, bf16[6,1024]{1,0:T(8,128)(2,1)S(1)}, u32[]{:S(2)}, u32[]{:S(2)}) %collective-permute-start.13) | collective-permute-done | bytes 12320 | tf_op jit(solution)/shard_map/ppermute | solution.py:14
  81.8 2.1 collective-permute-start.14
  83.9 3.5 collective-permute-done.14
  89.3 2.1 convolution_convert_fusion.4
  91.5 2.1 convolution_convert_fusion.3
  95.5 2.5 all-reduce
  98.1 27.2 %reduce-scatter.12.cloned.1.call-done = bf16[48,352]{1,0:T(8,128)(2,1)} async-done(((bf16[96,352]{1,0:T(8,128)(2,1)}), bf16[48,352]{1,0:T(8,128)(2,1)}) %reduce-scatter.12.cloned.1.call-update) | async-done | bytes 33808 | tf_op jit(solution)/shard_map/reduce_scatter | solution.py:24
  125.3 11.5 %reduce-scatter.14.cloned.1.call-done = bf16[48,352]{1,0:T(8,128)(2,1)} async-done(((bf16[96,352]{1,0:T(8,128)(2,1)}), bf16[48,352]{1,0:T(8,128)(2,1)}) %reduce-scatter.14.cloned.1.call-update) | async-done | bytes 33808 | tf_op jit(solution)/shard_map/reduce_scatter | solution.py:27
  139.8 35.6 %fusion = f32[8,1024]{1,0:T(8,128)S(1)} fusion(f32[96,1024]{1,0:T(8,128)S(1)} %fusion.47), kind=kCustom, calls=%all-reduce-scatter | all-reduce-scatter fusion | flops 131073 | bytes 426496
  175.4 6.0 %collective-permute-start.32 = (f32[8,1024]{1,0:T(8,128)S(1)}, f32[8,1024]{1,0:T(8,128)S(1)}, u32[]{:S(2)}, u32[]{:S(2)}) collective-permute-start(f32[8,1024]{1,0:T(8,128)S(1)} %fusion), channel_id=1, source_target_pairs={{0,6},{2,8},{4,10},{6,12},{8,14},{10,16},{12,18},{14,20},{16,22},{... | collective-permute-start | bytes 98312
  181.4 4.3 collective-permute-start.31
  185.8 4.9 collective-permute-start.30
  193.8 2.6 collective-permute-done.33
  199.5 5.1 %all-to-all-start = ((bf16[6,16,128]{2,0,1:T(8,128)(2,1)}), bf16[6,16,128]{2,0,1:T(8,128)(2,1)S(1)}, u32[]{:S(2)}, u32[]{:S(2)}) async-start(bf16[6,16,128]{2,0,1:T(8,128)(2,1)} %get-tuple-element.11), calls=%async_computation.2 | async-start | bytes 65536 | tf_op jit(solution)/shard_map/all_to_all | solution.py:64
  204.7 4.3 all-to-all-done
  210.4 52.3 %fusion.1 = f32[8,4096]{1,0:T(8,128)S(1)} fusion(f32[96,4096]{1,0:T(8,128)S(1)} %fusion.3), kind=kCustom, calls=%all-reduce-scatter.1 | all-reduce-scatter fusion | flops 524289 | bytes 1704448
  262.8 3.3 collective-permute-start.36
  266.0 3.0 collective-permute-start.35
  269.0 3.5 collective-permute-start.34
  274.5 4.9 collective-permute-done.37
  280.4 4.0 multiply_add_fusion
  286.1 2.8 fusion.48
  290.4 7.1 %reduce-scatter.16.cloned.1.call-done = bf16[6,1024]{1,0:T(8,128)(2,1)} async-done(((bf16[6,2048]{1,0:T(8,128)(2,1)}), bf16[6,1024]{1,0:T(8,128)(2,1)}) %reduce-scatter.16.cloned.1.call-update) | async-done | bytes 12304 | tf_op jit(solution)/shard_map/reduce_scatter | solution.py:102
  299.7 2.3 collective-permute-done.15
  301.9 2.4 collective-permute-start.16
  306.0 2.9 collective-permute-start.17
  308.9 2.6 collective-permute-done.17
  311.5 2.0 collective-permute-start.18
  313.6 3.5 collective-permute-done.18
  318.2 4.4 collective-permute-done.19
  322.9 5.3 %collective-permute-done.20 = bf16[6,1024]{1,0:T(8,128)(2,1)S(1)} collective-permute-done((bf16[6,1024]{1,0:T(8,128)(2,1)S(1)}, bf16[6,1024]{1,0:T(8,128)(2,1)S(1)}, u32[]{:S(2)}, u32[]{:S(2)}) %collective-permute-start.20) | collective-permute-done | bytes 12320 | tf_op jit(solution)/shard_map/ppermute | solution.py:14
  328.1 5.5 %collective-permute-done.21 = bf16[6,1024]{1,0:T(8,128)(2,1)S(1)} collective-permute-done((bf16[6,1024]{1,0:T(8,128)(2,1)S(1)}, bf16[6,1024]{1,0:T(8,128)(2,1)S(1)}, u32[]{:S(2)}, u32[]{:S(2)}) %collective-permute-start.21) | collective-permute-done | bytes 12320 | tf_op jit(solution)/shard_map/ppermute | solution.py:14
  333.7 5.5 %collective-permute-done.22 = bf16[6,1024]{1,0:T(8,128)(2,1)S(1)} collective-permute-done((bf16[6,1024]{1,0:T(8,128)(2,1)S(1)}, bf16[6,1024]{1,0:T(8,128)(2,1)S(1)}, u32[]{:S(2)}, u32[]{:S(2)}) %collective-permute-start.22) | collective-permute-done | bytes 12320 | tf_op jit(solution)/shard_map/ppermute | solution.py:14
  339.2 5.6 %collective-permute-done.23 = bf16[6,1024]{1,0:T(8,128)(2,1)S(1)} collective-permute-done((bf16[6,1024]{1,0:T(8,128)(2,1)S(1)}, bf16[6,1024]{1,0:T(8,128)(2,1)S(1)}, u32[]{:S(2)}, u32[]{:S(2)}) %collective-permute-start.23) | collective-permute-done | bytes 12320 | tf_op jit(solution)/shard_map/ppermute | solution.py:14
  344.8 5.5 %collective-permute-done.24 = bf16[6,1024]{1,0:T(8,128)(2,1)S(1)} collective-permute-done((bf16[6,1024]{1,0:T(8,128)(2,1)S(1)}, bf16[6,1024]{1,0:T(8,128)(2,1)S(1)}, u32[]{:S(2)}, u32[]{:S(2)}) %collective-permute-start.24) | collective-permute-done | bytes 12320 | tf_op jit(solution)/shard_map/ppermute | solution.py:14
  350.4 5.5 %collective-permute-done.25 = bf16[6,1024]{1,0:T(8,128)(2,1)S(1)} collective-permute-done((bf16[6,1024]{1,0:T(8,128)(2,1)S(1)}, bf16[6,1024]{1,0:T(8,128)(2,1)S(1)}, u32[]{:S(2)}, u32[]{:S(2)}) %collective-permute-start.25) | collective-permute-done | bytes 12320 | tf_op jit(solution)/shard_map/ppermute | solution.py:14
  355.9 5.5 %collective-permute-done.26 = bf16[6,1024]{1,0:T(8,128)(2,1)S(1)} collective-permute-done((bf16[6,1024]{1,0:T(8,128)(2,1)S(1)}, bf16[6,1024]{1,0:T(8,128)(2,1)S(1)}, u32[]{:S(2)}, u32[]{:S(2)}) %collective-permute-start.26) | collective-permute-done | bytes 12320 | tf_op jit(solution)/shard_map/ppermute | solution.py:14
  361.4 5.6 %collective-permute-done.27 = bf16[6,1024]{1,0:T(8,128)(2,1)S(1)} collective-permute-done((bf16[6,1024]{1,0:T(8,128)(2,1)S(1)}, bf16[6,1024]{1,0:T(8,128)(2,1)S(1)}, u32[]{:S(2)}, u32[]{:S(2)}) %collective-permute-start.27) | collective-permute-done | bytes 12320 | tf_op jit(solution)/shard_map/ppermute | solution.py:14
  367.3 5.3 %collective-permute-done.28 = bf16[6,1024]{1,0:T(8,128)(2,1)S(1)} collective-permute-done((bf16[6,1024]{1,0:T(8,128)(2,1)S(1)}, bf16[6,1024]{1,0:T(8,128)(2,1)S(1)}, u32[]{:S(2)}, u32[]{:S(2)}) %collective-permute-start.28) | collective-permute-done | bytes 12320 | tf_op jit(solution)/shard_map/ppermute | solution.py:14
  372.6 2.0 collective-permute-start.29
  374.6 3.5 collective-permute-done.29
  381.5 2.5 all-reduce.3
  384.0 30.1 %reduce-scatter.18.cloned.1.call-done = bf16[48,352]{1,0:T(8,128)(2,1)} async-done(((bf16[96,352]{1,0:T(8,128)(2,1)}), bf16[48,352]{1,0:T(8,128)(2,1)}) %reduce-scatter.18.cloned.1.call-update) | async-done | bytes 33808 | tf_op jit(solution)/shard_map/reduce_scatter | solution.py:24
  414.1 10.7 %reduce-scatter.20.cloned.1.call-done = bf16[48,352]{1,0:T(8,128)(2,1)} async-done(((bf16[96,352]{1,0:T(8,128)(2,1)}), bf16[48,352]{1,0:T(8,128)(2,1)}) %reduce-scatter.20.cloned.1.call-update) | async-done | bytes 33808 | tf_op jit(solution)/shard_map/reduce_scatter | solution.py:27
  427.9 35.6 %fusion.2 = f32[8,1024]{1,0:T(8,128)S(1)} fusion(f32[96,1024]{1,0:T(8,128)S(1)} %fusion.49), kind=kCustom, calls=%all-reduce-scatter.2 | all-reduce-scatter fusion | flops 131073 | bytes 426496
  463.4 6.0 %collective-permute-start.40 = (f32[8,1024]{1,0:T(8,128)S(1)}, f32[8,1024]{1,0:T(8,128)S(1)}, u32[]{:S(2)}, u32[]{:S(2)}) collective-permute-start(f32[8,1024]{1,0:T(8,128)S(1)} %fusion.2), channel_id=1, source_target_pairs={{0,6},{2,8},{4,10},{6,12},{8,14},{10,16},{12,18},{14,20},{16,22},{... | collective-permute-start | bytes 98312
  469.4 4.4 collective-permute-start.39
  473.8 4.9 collective-permute-start.38
  480.6 3.9 collective-permute-done.41
  (113 shorter events, 39.6 us)
Async XLA Ops:
  7.2 132.4 %copy-start = (bf16[352,1024]{1,0:T(8,128)(2,1)S(1)}, bf16[352,1024]{1,0:T(8,128)(2,1)}, u32[]{:S(2)}) copy-start(bf16[352,1024]{1,0:T(8,128)(2,1)} %param.24) | copy-start | bytes 2162692
  7.2 185.4 %copy-start.11 = (u32[32]{0:T(128)S(1)}, u32[32]{0:T(128)}, u32[]{:S(2)}) copy-start(u32[32]{0:T(128)} %constant.61) | copy-start | bytes 388
  7.2 189.7 %copy-start.6 = (bf16[6,1024]{1,0:T(8,128)(2,1)S(1)}, bf16[6,1024]{1,0:T(8,128)(2,1)}, u32[]{:S(2)}) copy-start(bf16[6,1024]{1,0:T(8,128)(2,1)} %param.20) | copy-start | bytes 36868
  7.2 191.6 %copy-start.8 = (f32[2048]{0:T(1024)S(1)}, f32[2048]{0:T(1024)}, u32[]{:S(2)}) copy-start(f32[2048]{0:T(1024)} %param.25) | copy-start | bytes 24580
  7.2 197.5 %copy-start.10 = (f32[1024]{0:T(1024)S(1)}, f32[1024]{0:T(1024)}, u32[]{:S(2)}) copy-start(f32[1024]{0:T(1024)} %param.30) | copy-start | bytes 12292
  7.2 201.8 %copy-start.12 = (bf16[128,1024]{1,0:T(8,128)(2,1)S(1)}, bf16[128,1024]{1,0:T(8,128)(2,1)}, u32[]{:S(2)}) copy-start(bf16[128,1024]{1,0:T(8,128)(2,1)} %param.29) | copy-start | bytes 786436
  7.2 201.8 %copy-start.13 = (bf16[128,1024]{1,0:T(8,128)(2,1)S(1)}, bf16[128,1024]{1,0:T(8,128)(2,1)}, u32[]{:S(2)}) copy-start(bf16[128,1024]{1,0:T(8,128)(2,1)} %param.28) | copy-start | bytes 786436
  7.2 118.1 %reduce-scatter.12.cloned.1.call-start = ((), (), s32[]{:S(2)}) async-start(), calls=%async_computation.6 | async-start | bytes 110592 | tf_op jit(solution)/shard_map/reduce_scatter | solution.py:24
  7.3 4.0 collective-permute-start
  11.3 4.0 collective-permute-start.1
  15.3 5.5 %collective-permute-start.2 = (bf16[6,1024]{1,0:T(8,128)(2,1)S(1)}, bf16[6,1024]{1,0:T(8,128)(2,1)S(1)}, u32[]{:S(2)}, u32[]{:S(2)}) collective-permute-start(bf16[6,1024]{1,0:T(8,128)(2,1)S(1)} %collective-permute-done.1), channel_id=1, source_target_pairs={{0,2},{2,4},{4,6},{6,8},{8,10},{10,12},{12,14},{14,16},{16,18},{18... | collective-permute-start | bytes 36872 | tf_op jit(solution)/shard_map/ppermute | solution.py:14
  20.9 5.6 %collective-permute-start.3 = (bf16[6,1024]{1,0:T(8,128)(2,1)S(1)}, bf16[6,1024]{1,0:T(8,128)(2,1)S(1)}, u32[]{:S(2)}, u32[]{:S(2)}) collective-permute-start(bf16[6,1024]{1,0:T(8,128)(2,1)S(1)} %collective-permute-done.2), channel_id=1, source_target_pairs={{0,2},{2,4},{4,6},{6,8},{8,10},{10,12},{12,14},{14,16},{16,18},{18... | collective-permute-start | bytes 36872 | tf_op jit(solution)/shard_map/ppermute | solution.py:14
  26.5 5.4 %collective-permute-start.4 = (bf16[6,1024]{1,0:T(8,128)(2,1)S(1)}, bf16[6,1024]{1,0:T(8,128)(2,1)S(1)}, u32[]{:S(2)}, u32[]{:S(2)}) collective-permute-start(bf16[6,1024]{1,0:T(8,128)(2,1)S(1)} %collective-permute-done.3), channel_id=1, source_target_pairs={{0,2},{2,4},{4,6},{6,8},{8,10},{10,12},{12,14},{14,16},{16,18},{18... | collective-permute-start | bytes 36872 | tf_op jit(solution)/shard_map/ppermute | solution.py:14
  32.0 5.5 %collective-permute-start.5 = (bf16[6,1024]{1,0:T(8,128)(2,1)S(1)}, bf16[6,1024]{1,0:T(8,128)(2,1)S(1)}, u32[]{:S(2)}, u32[]{:S(2)}) collective-permute-start(bf16[6,1024]{1,0:T(8,128)(2,1)S(1)} %collective-permute-done.4), channel_id=1, source_target_pairs={{0,2},{2,4},{4,6},{6,8},{8,10},{10,12},{12,14},{14,16},{16,18},{18... | collective-permute-start | bytes 36872 | tf_op jit(solution)/shard_map/ppermute | solution.py:14
  37.5 5.5 %collective-permute-start.6 = (bf16[6,1024]{1,0:T(8,128)(2,1)S(1)}, bf16[6,1024]{1,0:T(8,128)(2,1)S(1)}, u32[]{:S(2)}, u32[]{:S(2)}) collective-permute-start(bf16[6,1024]{1,0:T(8,128)(2,1)S(1)} %collective-permute-done.5), channel_id=1, source_target_pairs={{0,2},{2,4},{4,6},{6,8},{8,10},{10,12},{12,14},{14,16},{16,18},{18... | collective-permute-start | bytes 36872 | tf_op jit(solution)/shard_map/ppermute | solution.py:14
  43.0 5.6 %collective-permute-start.7 = (bf16[6,1024]{1,0:T(8,128)(2,1)S(1)}, bf16[6,1024]{1,0:T(8,128)(2,1)S(1)}, u32[]{:S(2)}, u32[]{:S(2)}) collective-permute-start(bf16[6,1024]{1,0:T(8,128)(2,1)S(1)} %collective-permute-done.6), channel_id=1, source_target_pairs={{0,2},{2,4},{4,6},{6,8},{8,10},{10,12},{12,14},{14,16},{16,18},{18... | collective-permute-start | bytes 36872 | tf_op jit(solution)/shard_map/ppermute | solution.py:14
  48.6 5.5 %collective-permute-start.8 = (bf16[6,1024]{1,0:T(8,128)(2,1)S(1)}, bf16[6,1024]{1,0:T(8,128)(2,1)S(1)}, u32[]{:S(2)}, u32[]{:S(2)}) collective-permute-start(bf16[6,1024]{1,0:T(8,128)(2,1)S(1)} %collective-permute-done.7), channel_id=1, source_target_pairs={{0,2},{2,4},{4,6},{6,8},{8,10},{10,12},{12,14},{14,16},{16,18},{18... | collective-permute-start | bytes 36872 | tf_op jit(solution)/shard_map/ppermute | solution.py:14
  54.1 5.5 %collective-permute-start.9 = (bf16[6,1024]{1,0:T(8,128)(2,1)S(1)}, bf16[6,1024]{1,0:T(8,128)(2,1)S(1)}, u32[]{:S(2)}, u32[]{:S(2)}) collective-permute-start(bf16[6,1024]{1,0:T(8,128)(2,1)S(1)} %collective-permute-done.8), channel_id=1, source_target_pairs={{0,2},{2,4},{4,6},{6,8},{8,10},{10,12},{12,14},{14,16},{16,18},{18... | collective-permute-start | bytes 36872 | tf_op jit(solution)/shard_map/ppermute | solution.py:14
  59.6 5.5 %collective-permute-start.10 = (bf16[6,1024]{1,0:T(8,128)(2,1)S(1)}, bf16[6,1024]{1,0:T(8,128)(2,1)S(1)}, u32[]{:S(2)}, u32[]{:S(2)}) collective-permute-start(bf16[6,1024]{1,0:T(8,128)(2,1)S(1)} %collective-permute-done.9), channel_id=1, source_target_pairs={{0,2},{2,4},{4,6},{6,8},{8,10},{10,12},{12,14},{14,16},{16,18},{18... | collective-permute-start | bytes 36872 | tf_op jit(solution)/shard_map/ppermute | solution.py:14
  65.2 5.5 %collective-permute-start.11 = (bf16[6,1024]{1,0:T(8,128)(2,1)S(1)}, bf16[6,1024]{1,0:T(8,128)(2,1)S(1)}, u32[]{:S(2)}, u32[]{:S(2)}) collective-permute-start(bf16[6,1024]{1,0:T(8,128)(2,1)S(1)} %collective-permute-done.10), channel_id=1, source_target_pairs={{0,2},{2,4},{4,6},{6,8},{8,10},{10,12},{12,14},{14,16},{16,18},{18... | collective-permute-start | bytes 36872 | tf_op jit(solution)/shard_map/ppermute | solution.py:14
  70.7 5.5 %collective-permute-start.12 = (bf16[6,1024]{1,0:T(8,128)(2,1)S(1)}, bf16[6,1024]{1,0:T(8,128)(2,1)S(1)}, u32[]{:S(2)}, u32[]{:S(2)}) collective-permute-start(bf16[6,1024]{1,0:T(8,128)(2,1)S(1)} %collective-permute-done.11), channel_id=1, source_target_pairs={{0,2},{2,4},{4,6},{6,8},{8,10},{10,12},{12,14},{14,16},{16,18},{18... | collective-permute-start | bytes 36872 | tf_op jit(solution)/shard_map/ppermute | solution.py:14
  76.3 5.5 %collective-permute-start.13 = (bf16[6,1024]{1,0:T(8,128)(2,1)S(1)}, bf16[6,1024]{1,0:T(8,128)(2,1)S(1)}, u32[]{:S(2)}, u32[]{:S(2)}) collective-permute-start(bf16[6,1024]{1,0:T(8,128)(2,1)S(1)} %collective-permute-done.12), channel_id=1, source_target_pairs={{0,2},{2,4},{4,6},{6,8},{8,10},{10,12},{12,14},{14,16},{16,18},{18... | collective-permute-start | bytes 36872 | tf_op jit(solution)/shard_map/ppermute | solution.py:14
  81.8 5.5 %collective-permute-start.14 = (bf16[6,1024]{1,0:T(8,128)(2,1)S(1)}, bf16[6,1024]{1,0:T(8,128)(2,1)S(1)}, u32[]{:S(2)}, u32[]{:S(2)}) collective-permute-start(bf16[6,1024]{1,0:T(8,128)(2,1)S(1)} %collective-permute-done.13), channel_id=1, source_target_pairs={{0,2},{2,4},{4,6},{6,8},{8,10},{10,12},{12,14},{14,16},{16,18},{18... | collective-permute-start | bytes 36872 | tf_op jit(solution)/shard_map/ppermute | solution.py:14
  91.4 45.4 %reduce-scatter.14.cloned.1.call-start = ((), (), s32[]{:S(2)}) async-start(), calls=%async_computation.7 | async-start | bytes 110592 | tf_op jit(solution)/shard_map/reduce_scatter | solution.py:27
  175.4 21.1 %collective-permute-start.32 = (f32[8,1024]{1,0:T(8,128)S(1)}, f32[8,1024]{1,0:T(8,128)S(1)}, u32[]{:S(2)}, u32[]{:S(2)}) collective-permute-start(f32[8,1024]{1,0:T(8,128)S(1)} %fusion), channel_id=1, source_target_pairs={{0,6},{2,8},{4,10},{6,12},{8,14},{10,16},{12,18},{14,20},{16,22},{... | collective-permute-start | bytes 98312
  181.4 15.1 %collective-permute-start.31 = (f32[8,1024]{1,0:T(8,128)S(1)}, f32[8,1024]{1,0:T(8,128)S(1)}, u32[]{:S(2)}, u32[]{:S(2)}) collective-permute-start(f32[8,1024]{1,0:T(8,128)S(1)} %fusion), channel_id=1, source_target_pairs={{0,4},{2,6},{4,8},{6,10},{8,12},{10,14},{12,16},{14,18},{16,20},{1... | collective-permute-start | bytes 98312
  185.8 10.7 %collective-permute-start.30 = (f32[8,1024]{1,0:T(8,128)S(1)}, f32[8,1024]{1,0:T(8,128)S(1)}, u32[]{:S(2)}, u32[]{:S(2)}) collective-permute-start(f32[8,1024]{1,0:T(8,128)S(1)} %fusion), channel_id=1, source_target_pairs={{0,2},{2,4},{4,6},{6,8},{8,10},{10,12},{12,14},{14,16},{16,18},{18... | collective-permute-start | bytes 98312
  190.7 5.8 %collective-permute-start.33 = (f32[6,1024]{1,0:T(8,128)S(1)}, f32[6,1024]{1,0:T(8,128)S(1)}, u32[]{:S(2)}, u32[]{:S(2)}) collective-permute-start(f32[6,1024]{1,0:T(8,128)S(1)} %slice.20), channel_id=1, source_target_pairs={{0,8},{2,10},{4,12},{6,14},{8,16},{10,18},{12,20},{14,22},{16,24},... | collective-permute-start | bytes 73736
  199.5 9.4 %all-to-all-start = ((bf16[6,16,128]{2,0,1:T(8,128)(2,1)}), bf16[6,16,128]{2,0,1:T(8,128)(2,1)S(1)}, u32[]{:S(2)}, u32[]{:S(2)}) async-start(bf16[6,16,128]{2,0,1:T(8,128)(2,1)} %get-tuple-element.11), calls=%async_computation.2 | async-start | bytes 65536 | tf_op jit(solution)/shard_map/all_to_all | solution.py:64
  204.7 92.8 %reduce-scatter.16.cloned.1.call-start = ((), (), s32[]{:S(2)}) async-start(), calls=%async_computation.8 | async-start | bytes 49152 | tf_op jit(solution)/shard_map/reduce_scatter | solution.py:102
  262.8 16.6 %collective-permute-start.36 = (f32[8,4096]{1,0:T(8,128)S(1)}, f32[8,4096]{1,0:T(8,128)S(1)}, u32[]{:S(2)}, u32[]{:S(2)}) collective-permute-start(f32[8,4096]{1,0:T(8,128)S(1)} %fusion.1), channel_id=1, source_target_pairs={{0,6},{2,8},{4,10},{6,12},{8,14},{10,16},{12,18},{14,20},{16,22},{... | collective-permute-start | bytes 393224
  266.0 13.4 %collective-permute-start.35 = (f32[8,4096]{1,0:T(8,128)S(1)}, f32[8,4096]{1,0:T(8,128)S(1)}, u32[]{:S(2)}, u32[]{:S(2)}) collective-permute-start(f32[8,4096]{1,0:T(8,128)S(1)} %fusion.1), channel_id=1, source_target_pairs={{0,4},{2,6},{4,8},{6,10},{8,12},{10,14},{12,16},{14,18},{16,20},{1... | collective-permute-start | bytes 393224
  269.0 10.4 %collective-permute-start.34 = (f32[8,4096]{1,0:T(8,128)S(1)}, f32[8,4096]{1,0:T(8,128)S(1)}, u32[]{:S(2)}, u32[]{:S(2)}) collective-permute-start(f32[8,4096]{1,0:T(8,128)S(1)} %fusion.1), channel_id=1, source_target_pairs={{0,2},{2,4},{4,6},{6,8},{8,10},{10,12},{12,14},{14,16},{16,18},{18... | collective-permute-start | bytes 393224
  272.5 6.9 %collective-permute-start.37 = (f32[6,4096]{1,0:T(8,128)S(1)}, f32[6,4096]{1,0:T(8,128)S(1)}, u32[]{:S(2)}, u32[]{:S(2)}) collective-permute-start(f32[6,4096]{1,0:T(8,128)S(1)} %slice.21), channel_id=1, source_target_pairs={{0,8},{2,10},{4,12},{6,14},{8,16},{10,18},{12,20},{14,22},{16,24},... | collective-permute-start | bytes 294920
  280.4 8.6 %copy-start.2 = (bf16[1024,2048]{1,0:T(8,128)(2,1)S(1)}, bf16[1024,2048]{1,0:T(8,128)(2,1)}, u32[]{:S(2)}) copy-start(bf16[1024,2048]{1,0:T(8,128)(2,1)} %param.32) | copy-start | bytes 12582916
  284.4 1.7 copy-start.1
  284.4 4.5 copy-start.9
  288.8 90.6 %copy-start.4 = (bf16[1024,352]{0,1:T(8,128)(2,1)S(1)}, bf16[1024,352]{0,1:T(8,128)(2,1)}, u32[]{:S(2)}) copy-start(bf16[1024,352]{0,1:T(8,128)(2,1)} %param.34) | copy-start | bytes 2162692
  288.8 90.6 %copy-start.7 = (f32[1024]{0:T(1024)S(1)}, f32[1024]{0:T(1024)}, u32[]{:S(2)}) copy-start(f32[1024]{0:T(1024)} %param.33) | copy-start | bytes 12292
  289.0 91.4 %copy-start.5 = (bf16[1024,352]{0,1:T(8,128)(2,1)S(1)}, bf16[1024,352]{0,1:T(8,128)(2,1)}, u32[]{:S(2)}) copy-start(bf16[1024,352]{0,1:T(8,128)(2,1)} %param.35) | copy-start | bytes 2162692
  289.0 138.5 %copy-start.3 = (bf16[352,1024]{1,0:T(8,128)(2,1)S(1)}, bf16[352,1024]{1,0:T(8,128)(2,1)}, u32[]{:S(2)}) copy-start(bf16[352,1024]{1,0:T(8,128)(2,1)} %param.36) | copy-start | bytes 2162692
  290.3 123.8 %reduce-scatter.18.cloned.1.call-start = ((), (), s32[]{:S(2)}) async-start(), calls=%async_computation.9 | async-start | bytes 110592 | tf_op jit(solution)/shard_map/reduce_scatter | solution.py:24
  298.2 3.7 collective-permute-start.15
  301.9 4.1 collective-permute-start.16
  306.0 5.5 %collective-permute-start.17 = (bf16[6,1024]{1,0:T(8,128)(2,1)S(1)}, bf16[6,1024]{1,0:T(8,128)(2,1)S(1)}, u32[]{:S(2)}, u32[]{:S(2)}) collective-permute-start(bf16[6,1024]{1,0:T(8,128)(2,1)S(1)} %collective-permute-done.16), channel_id=1, source_target_pairs={{0,2},{2,4},{4,6},{6,8},{8,10},{10,12},{12,14},{14,16},{16,18},{18... | collective-permute-start | bytes 36872 | tf_op jit(solution)/shard_map/ppermute | solution.py:14
  311.5 5.5 %collective-permute-start.18 = (bf16[6,1024]{1,0:T(8,128)(2,1)S(1)}, bf16[6,1024]{1,0:T(8,128)(2,1)S(1)}, u32[]{:S(2)}, u32[]{:S(2)}) collective-permute-start(bf16[6,1024]{1,0:T(8,128)(2,1)S(1)} %collective-permute-done.17), channel_id=1, source_target_pairs={{0,2},{2,4},{4,6},{6,8},{8,10},{10,12},{12,14},{14,16},{16,18},{18... | collective-permute-start | bytes 36872 | tf_op jit(solution)/shard_map/ppermute | solution.py:14
  317.1 5.5 %collective-permute-start.19 = (bf16[6,1024]{1,0:T(8,128)(2,1)S(1)}, bf16[6,1024]{1,0:T(8,128)(2,1)S(1)}, u32[]{:S(2)}, u32[]{:S(2)}) collective-permute-start(bf16[6,1024]{1,0:T(8,128)(2,1)S(1)} %collective-permute-done.18), channel_id=1, source_target_pairs={{0,2},{2,4},{4,6},{6,8},{8,10},{10,12},{12,14},{14,16},{16,18},{18... | collective-permute-start | bytes 36872 | tf_op jit(solution)/shard_map/ppermute | solution.py:14
  322.6 5.5 %collective-permute-start.20 = (bf16[6,1024]{1,0:T(8,128)(2,1)S(1)}, bf16[6,1024]{1,0:T(8,128)(2,1)S(1)}, u32[]{:S(2)}, u32[]{:S(2)}) collective-permute-start(bf16[6,1024]{1,0:T(8,128)(2,1)S(1)} %collective-permute-done.19), channel_id=1, source_target_pairs={{0,2},{2,4},{4,6},{6,8},{8,10},{10,12},{12,14},{14,16},{16,18},{18... | collective-permute-start | bytes 36872 | tf_op jit(solution)/shard_map/ppermute | solution.py:14
  328.1 5.5 %collective-permute-start.21 = (bf16[6,1024]{1,0:T(8,128)(2,1)S(1)}, bf16[6,1024]{1,0:T(8,128)(2,1)S(1)}, u32[]{:S(2)}, u32[]{:S(2)}) collective-permute-start(bf16[6,1024]{1,0:T(8,128)(2,1)S(1)} %collective-permute-done.20), channel_id=1, source_target_pairs={{0,2},{2,4},{4,6},{6,8},{8,10},{10,12},{12,14},{14,16},{16,18},{18... | collective-permute-start | bytes 36872 | tf_op jit(solution)/shard_map/ppermute | solution.py:14
  333.7 5.5 %collective-permute-start.22 = (bf16[6,1024]{1,0:T(8,128)(2,1)S(1)}, bf16[6,1024]{1,0:T(8,128)(2,1)S(1)}, u32[]{:S(2)}, u32[]{:S(2)}) collective-permute-start(bf16[6,1024]{1,0:T(8,128)(2,1)S(1)} %collective-permute-done.21), channel_id=1, source_target_pairs={{0,2},{2,4},{4,6},{6,8},{8,10},{10,12},{12,14},{14,16},{16,18},{18... | collective-permute-start | bytes 36872 | tf_op jit(solution)/shard_map/ppermute | solution.py:14
  339.2 5.6 %collective-permute-start.23 = (bf16[6,1024]{1,0:T(8,128)(2,1)S(1)}, bf16[6,1024]{1,0:T(8,128)(2,1)S(1)}, u32[]{:S(2)}, u32[]{:S(2)}) collective-permute-start(bf16[6,1024]{1,0:T(8,128)(2,1)S(1)} %collective-permute-done.22), channel_id=1, source_target_pairs={{0,2},{2,4},{4,6},{6,8},{8,10},{10,12},{12,14},{14,16},{16,18},{18... | collective-permute-start | bytes 36872 | tf_op jit(solution)/shard_map/ppermute | solution.py:14
  344.8 5.5 %collective-permute-start.24 = (bf16[6,1024]{1,0:T(8,128)(2,1)S(1)}, bf16[6,1024]{1,0:T(8,128)(2,1)S(1)}, u32[]{:S(2)}, u32[]{:S(2)}) collective-permute-start(bf16[6,1024]{1,0:T(8,128)(2,1)S(1)} %collective-permute-done.23), channel_id=1, source_target_pairs={{0,2},{2,4},{4,6},{6,8},{8,10},{10,12},{12,14},{14,16},{16,18},{18... | collective-permute-start | bytes 36872 | tf_op jit(solution)/shard_map/ppermute | solution.py:14
  350.4 5.5 %collective-permute-start.25 = (bf16[6,1024]{1,0:T(8,128)(2,1)S(1)}, bf16[6,1024]{1,0:T(8,128)(2,1)S(1)}, u32[]{:S(2)}, u32[]{:S(2)}) collective-permute-start(bf16[6,1024]{1,0:T(8,128)(2,1)S(1)} %collective-permute-done.24), channel_id=1, source_target_pairs={{0,2},{2,4},{4,6},{6,8},{8,10},{10,12},{12,14},{14,16},{16,18},{18... | collective-permute-start | bytes 36872 | tf_op jit(solution)/shard_map/ppermute | solution.py:14
  355.9 5.5 %collective-permute-start.26 = (bf16[6,1024]{1,0:T(8,128)(2,1)S(1)}, bf16[6,1024]{1,0:T(8,128)(2,1)S(1)}, u32[]{:S(2)}, u32[]{:S(2)}) collective-permute-start(bf16[6,1024]{1,0:T(8,128)(2,1)S(1)} %collective-permute-done.25), channel_id=1, source_target_pairs={{0,2},{2,4},{4,6},{6,8},{8,10},{10,12},{12,14},{14,16},{16,18},{18... | collective-permute-start | bytes 36872 | tf_op jit(solution)/shard_map/ppermute | solution.py:14
  361.4 5.6 %collective-permute-start.27 = (bf16[6,1024]{1,0:T(8,128)(2,1)S(1)}, bf16[6,1024]{1,0:T(8,128)(2,1)S(1)}, u32[]{:S(2)}, u32[]{:S(2)}) collective-permute-start(bf16[6,1024]{1,0:T(8,128)(2,1)S(1)} %collective-permute-done.26), channel_id=1, source_target_pairs={{0,2},{2,4},{4,6},{6,8},{8,10},{10,12},{12,14},{14,16},{16,18},{18... | collective-permute-start | bytes 36872 | tf_op jit(solution)/shard_map/ppermute | solution.py:14
  367.1 5.5 %collective-permute-start.28 = (bf16[6,1024]{1,0:T(8,128)(2,1)S(1)}, bf16[6,1024]{1,0:T(8,128)(2,1)S(1)}, u32[]{:S(2)}, u32[]{:S(2)}) collective-permute-start(bf16[6,1024]{1,0:T(8,128)(2,1)S(1)} %collective-permute-done.27), channel_id=1, source_target_pairs={{0,2},{2,4},{4,6},{6,8},{8,10},{10,12},{12,14},{14,16},{16,18},{18... | collective-permute-start | bytes 36872 | tf_op jit(solution)/shard_map/ppermute | solution.py:14
  372.6 5.5 %collective-permute-start.29 = (bf16[6,1024]{1,0:T(8,128)(2,1)S(1)}, bf16[6,1024]{1,0:T(8,128)(2,1)S(1)}, u32[]{:S(2)}, u32[]{:S(2)}) collective-permute-start(bf16[6,1024]{1,0:T(8,128)(2,1)S(1)} %collective-permute-done.28), channel_id=1, source_target_pairs={{0,2},{2,4},{4,6},{6,8},{8,10},{10,12},{12,14},{14,16},{16,18},{18... | collective-permute-start | bytes 36872 | tf_op jit(solution)/shard_map/ppermute | solution.py:14
  380.4 44.4 %reduce-scatter.20.cloned.1.call-start = ((), (), s32[]{:S(2)}) async-start(), calls=%async_computation.10 | async-start | bytes 110592 | tf_op jit(solution)/shard_map/reduce_scatter | solution.py:27
  463.4 21.1 %collective-permute-start.40 = (f32[8,1024]{1,0:T(8,128)S(1)}, f32[8,1024]{1,0:T(8,128)S(1)}, u32[]{:S(2)}, u32[]{:S(2)}) collective-permute-start(f32[8,1024]{1,0:T(8,128)S(1)} %fusion.2), channel_id=1, source_target_pairs={{0,6},{2,8},{4,10},{6,12},{8,14},{10,16},{12,18},{14,20},{16,22},{... | collective-permute-start | bytes 98312
  469.4 15.1 %collective-permute-start.39 = (f32[8,1024]{1,0:T(8,128)S(1)}, f32[8,1024]{1,0:T(8,128)S(1)}, u32[]{:S(2)}, u32[]{:S(2)}) collective-permute-start(f32[8,1024]{1,0:T(8,128)S(1)} %fusion.2), channel_id=1, source_target_pairs={{0,4},{2,6},{4,8},{6,10},{8,12},{10,14},{12,16},{14,18},{16,20},{1... | collective-permute-start | bytes 98312
  473.8 10.7 %collective-permute-start.38 = (f32[8,1024]{1,0:T(8,128)S(1)}, f32[8,1024]{1,0:T(8,128)S(1)}, u32[]{:S(2)}, u32[]{:S(2)}) collective-permute-start(f32[8,1024]{1,0:T(8,128)S(1)} %fusion.2), channel_id=1, source_target_pairs={{0,2},{2,4},{4,6},{6,8},{8,10},{10,12},{12,14},{14,16},{16,18},{18... | collective-permute-start | bytes 98312
  478.7 5.8 %collective-permute-start.41 = (f32[6,1024]{1,0:T(8,128)S(1)}, f32[6,1024]{1,0:T(8,128)S(1)}, u32[]{:S(2)}, u32[]{:S(2)}) collective-permute-start(f32[6,1024]{1,0:T(8,128)S(1)} %slice.22), channel_id=1, source_target_pairs={{0,8},{2,10},{4,12},{6,14},{8,16},{10,18},{12,20},{14,22},{16,24},... | collective-permute-start | bytes 73736
Sparse Core Ops, SparseCore 0:
  91.6 33.6 reduce-scatter.11
  128.1 8.6 reduce-scatter.13
  290.5 6.9 reduce-scatter.15
  380.5 33.5 reduce-scatter.17
  416.1 8.6 reduce-scatter.19
